TPU v7x, 32 devices: a whole 2x2x4 slice. The times are simulated.
32 devices in a mesh: sp: 8 (over z, x), tp: 4 (over y, core).
Axes of the slice: x: 2, y: 2, z: 4, core: 2. Of those that a mesh axis runs over, the one named last changes fastest.
Arguments:
- tokens: bfloat16 [1024, 1024], P('sp', 'tp'), may hold values from -6 to 6
- norm_gain: float32 [3, 1024], replicated, may hold values from 0.1 to 1.9
- w_query: bfloat16 [3, 1024, 1024], P(None, 'sp', 'tp'), may hold values from -0.1875 to 0.1875
- w_key: bfloat16 [3, 1024, 1024], P(None, 'sp', 'tp'), may hold values from -0.1875 to 0.1875
- w_value: bfloat16 [3, 1024, 1024], P(None, 'sp', 'tp'), may hold values from -0.1875 to 0.1875
- w_out: bfloat16 [3, 1024, 1024], P(None, 'tp', 'sp'), may hold values from -0.5625 to 0.5625
- offset_bias: float32 [3, 16, 8, 16], P(None, 'tp'), may hold values from -3 to 3
- documents: int32 [1024], P('sp'), may hold values from 0 to 7, never falling along the last dimension, each value on 1 to 256 neighbouring positions
Outputs:
- mixed: bfloat16 [1024, 1024], P('sp', 'tp')
Inputs may be any that keep to these rules, and one draw needn't show every extreme that they name: `documents`: document numbers never fall along the token order, start at 0, and each document has 1 to 256 tokens.
All inputs are finite; a program needn't handle non-finite values.
Results may differ from a plain program's by a relative error of at most 0.02.
Values may be sent and summed in bfloat16 or wider, within the bound.
A program may use at most 64 MiB of HBM per device.

v0:
```python
import jax
import jax.numpy as jnp
from jax import lax
from jax.sharding import PartitionSpec as P

HEAD_DIM = 64
WIN_ROWS = 8
WIN_COLS = 16
LAYERS = 3
GRID_W = 32
EPS = 1e-06


def with_halo(shard, sides, width, wrap):
    for axis, dim in sides:
        count, length = (lax.axis_size(axis), shard.shape[dim])
        up = [(i, (i + 1) % count) for i in range(count if wrap else count - 1)]
        down = [(j, i) for i, j in up]
        last = lax.slice_in_dim(shard, length - width, length, axis=dim)
        leading = lax.slice_in_dim(shard, 0, width, axis=dim)
        before = lax.ppermute(last, axis, up)
        after = lax.ppermute(leading, axis, down)
        shard = jnp.concatenate([before, shard, after], axis=dim)
    return shard


def rms_rows(stream, gain_row):
    values = stream.astype(jnp.float32)
    mean_sq = jnp.mean(values * values, axis=-1, keepdims=True)
    return (values * lax.rsqrt(mean_sq + EPS) * gain_row).astype(jnp.bfloat16)


def head_norm(heads_raw):
    values = heads_raw.astype(jnp.float32)
    mean_sq = jnp.mean(values * values, axis=-1, keepdims=True)
    return (values * lax.rsqrt(mean_sq + EPS)).astype(jnp.bfloat16)


def attend(queries, fringe, seg_own, seg_fringe, bias_layer):
    row_count, grid_width, head_count, head_width = queries.shape
    key_rows = jnp.stack(
        [fringe[row_lag : row_lag + row_count] for row_lag in range(WIN_ROWS)], axis=1
    )
    seg_rows = jnp.stack(
        [seg_fringe[row_lag : row_lag + row_count] for row_lag in range(WIN_ROWS)], axis=1
    )
    key_part = key_rows[..., :head_width]
    value_part = key_rows[..., head_width:]
    scores = jnp.einsum(
        "rchd,rjkhd->rhcjk", queries, key_part, preferred_element_type=jnp.float32
    ) * head_width ** (-0.5)
    column = jnp.arange(grid_width)
    col_offset = column[None, :] - column[:, None] + WIN_COLS // 2
    inside = (col_offset >= 0) & (col_offset < WIN_COLS)
    bias_table = bias_layer[:, :, jnp.clip(col_offset, 0, WIN_COLS - 1)]
    scores = scores + jnp.transpose(bias_table, (0, 2, 1, 3))[None]
    same_doc = seg_rows[:, None, None, :, :] == seg_own[:, None, :, None, None]
    allowed = same_doc & inside[None, None, :, None, :]
    scores = jnp.where(allowed, scores, -1e30)
    flat = scores.reshape(row_count, head_count, grid_width, WIN_ROWS * grid_width)
    attn_probs = jax.nn.softmax(flat, axis=-1).astype(jnp.bfloat16)
    attn_probs = attn_probs.reshape(row_count, head_count, grid_width, WIN_ROWS, grid_width)
    mixed_heads = jnp.einsum(
        "rhcjk,rjkhd->rchd", attn_probs, value_part, preferred_element_type=jnp.float32
    )
    return mixed_heads.astype(jnp.bfloat16)


def body(tokens, norm_gain, w_query, w_key, w_value, w_out, offset_bias, documents):
    token_count = tokens.shape[0]
    row_count = token_count // GRID_W
    reach_rows = WIN_ROWS // 2
    head_count = offset_bias.shape[1]
    seg_own = (documents + 1).reshape(row_count, GRID_W)
    seg_fringe = with_halo(seg_own, (("sp", 0),), reach_rows, False)
    collected = (
        lax.all_gather(w_query, "sp", axis=1, tiled=True),
        lax.all_gather(w_key, "sp", axis=1, tiled=True),
        lax.all_gather(w_value, "sp", axis=1, tiled=True),
        lax.all_gather(w_out, "sp", axis=2, tiled=True),
    )
    stream = tokens
    for layer_index in range(LAYERS):
        gathered = lax.all_gather(stream, "tp", axis=1, tiled=True)
        normed = rms_rows(gathered, norm_gain[layer_index])
        query_raw = jnp.dot(normed, collected[0][layer_index], preferred_element_type=jnp.float32)
        key_raw = jnp.dot(normed, collected[1][layer_index], preferred_element_type=jnp.float32)
        value_raw = jnp.dot(normed, collected[2][layer_index], preferred_element_type=jnp.float32)
        query_heads = head_norm(
            query_raw.astype(jnp.bfloat16).reshape(row_count, GRID_W, head_count, HEAD_DIM)
        )
        key_heads = head_norm(
            key_raw.astype(jnp.bfloat16).reshape(row_count, GRID_W, head_count, HEAD_DIM)
        )
        value_heads = value_raw.astype(jnp.bfloat16).reshape(
            row_count, GRID_W, head_count, HEAD_DIM
        )
        key_value = jnp.concatenate([key_heads, value_heads], axis=-1)
        fringe = with_halo(key_value, (("sp", 0),), reach_rows, False)
        attended = attend(query_heads, fringe, seg_own, seg_fringe, offset_bias[layer_index])
        attended = attended.reshape(token_count, head_count * HEAD_DIM)
        partial_sums = jnp.dot(
            attended, collected[3][layer_index], preferred_element_type=jnp.float32
        )
        stream = (
            lax.psum_scatter(
                partial_sums.astype(jnp.bfloat16), "tp", scatter_dimension=1, tiled=True
            )
            .astype(jnp.float32)
            .astype(jnp.bfloat16)
        )
    return stream


def solution(mesh):
    return jax.shard_map(
        body,
        mesh=mesh,
        in_specs=(
            P("sp", "tp"),
            P(),
            P(None, "sp", "tp"),
            P(None, "sp", "tp"),
            P(None, "sp", "tp"),
            P(None, "tp", "sp"),
            P(None, "tp", None, None),
            P("sp"),
        ),
        out_specs=P("sp", "tp"),
        check_vma=False,
    )
```

profile of v0, /device:TPU:0, one launch (start us, length us, event | category | flops | bytes accessed | tf_op | source)
XLA Modules:
  0.0 309.1 jit_solution(167499018848324964)
XLA Ops:
  6.5 0.7 all-gather.5.cloned.1.call-update
  7.3 0.7 all-gather.7.cloned.1.call-update
  8.1 0.7 all-gather.9.cloned.1.call-update
  8.8 0.7 broadcast_add_fusion
  9.5 4.9 %collective-permute-start.2 = (s32[4,32]{1,0:T(4,128)S(1)}, s32[4,32]{1,0:T(4,128)S(1)}, u32[]{:S(2)}, u32[]{:S(2)}) collective-permute-start(s32[4,32]{1,0:T(4,128)S(1)} %reshape.186), channel_id=1, source_target_pairs={{0,4},{4,8},{8,12},{12,16},{16,20},{20,24},{24,28},{1,5},{5,9},{9,... | collective-permute-start | bytes 1544 | tf_op jit(solution)/shard_map/ppermute | solution.py:21
  14.4 1.3 collective-permute-start.3
  15.8 6.0 %all_gather.21 = bf16[128,1024]{1,0:T(8,128)(2,1)S(1)} all-gather(bf16[128,256]{1,0:T(8,128)(2,1)} %param.8), channel_id=1, replica_groups=mesh['sp'=8,'tp'=4] {'tp'}, dimensions={1}, use_global_device_ids=true | all-gather | bytes 327680 | tf_op jit(solution)/shard_map/all_gather | solution.py:84
  21.9 0.8 fusion.79
  22.8 0.8 fusion.78
  23.8 3.5 %gather_fusion = f32[1024,4,8]{2,1,0:T(4,128)S(1)} fusion(f32[4,8,16]{1,0,2:T(4,128)S(1)} %bitcast.251, s32[1024]{0:T(1024)S(1)} %broadcast_clamp_fusion), kind=kCustom, calls=%fused_computation | custom fusion | bytes 266240 | tf_op jit(solution)/shard_map/gather | solution.py:55
  27.3 1.3 copy.150
  28.7 0.2 compare_and_fusion
  29.0 27.4 %all-gather.5.cloned.1.call-done = bf16[3,1024,256]{2,1,0:T(8,128)(2,1)} async-done(((bf16[3,128,256]{2,1,0:T(8,128)(2,1)}), bf16[3,1024,256]{2,1,0:T(8,128)(2,1)}) %all-gather.5.cloned.1.call-update) | async-done | bytes 1572880 | tf_op jit(solution)/shard_map/all_gather | solution.py:78
  56.4 1.3 fusion.17
  57.7 0.2 reshape.192
  57.9 0.2 multiply_reduce_fusion.5
  58.4 42.8 %all-gather.7.cloned.1.call-done = bf16[3,1024,256]{2,1,0:T(8,128)(2,1)} async-done(((bf16[3,128,256]{2,1,0:T(8,128)(2,1)}), bf16[3,1024,256]{2,1,0:T(8,128)(2,1)}) %all-gather.7.cloned.1.call-update) | async-done | bytes 1572880 | tf_op jit(solution)/shard_map/all_gather | solution.py:79
  101.2 1.3 convolution_convert_fusion.10
  102.8 2.5 collective-permute-start
  105.2 1.3 collective-permute-start.1
  106.5 39.4 %all-gather.9.cloned.1.call-done = bf16[3,1024,256]{2,1,0:T(8,128)(2,1)} async-done(((bf16[3,128,256]{2,1,0:T(8,128)(2,1)}), bf16[3,1024,256]{2,1,0:T(8,128)(2,1)}) %all-gather.9.cloned.1.call-update) | async-done | bytes 1572880 | tf_op jit(solution)/shard_map/all_gather | solution.py:77
  146.0 1.3 fusion.16
  147.4 0.2 multiply_reduce_fusion.4
  147.7 0.2 multiply_convert_fusion.2
  148.3 0.7 fusion.3
  148.9 0.6 fusion
  149.5 1.1 fusion.11
  150.8 39.8 %all-gather.11.cloned.1.call-done = bf16[3,256,1024]{2,1,0:T(8,128)(2,1)} async-done(((bf16[3,256,128]{2,1,0:T(8,128)(2,1)}), bf16[3,256,1024]{2,1,0:T(8,128)(2,1)}) %all-gather.11.cloned.1.call-update) | async-done | bytes 1572880 | tf_op jit(solution)/shard_map/all_gather | solution.py:80
  190.7 2.0 convolution_convert_fusion.2
  192.8 3.6 %gather_fusion.1 = f32[1024,4,8]{2,1,0:T(4,128)S(1)} fusion(f32[4,8,16]{1,0,2:T(4,128)S(1)} %bitcast.252, s32[1024]{0:T(1024)S(1)} %broadcast_clamp_fusion), kind=kCustom, calls=%fused_computation.1 | custom fusion | bytes 266240 | tf_op jit(solution)/shard_map/gather | solution.py:55
  196.4 1.3 copy.167
  197.6 13.6 %reduce-scatter.4.cloned.1.call-done = bf16[128,256]{1,0:T(8,128)(2,1)} async-done(((bf16[128,1024]{1,0:T(8,128)(2,1)}), bf16[128,256]{1,0:T(8,128)(2,1)}) %reduce-scatter.4.cloned.1.call-update) | async-done | bytes 65552 | tf_op jit(solution)/shard_map/reduce_scatter | solution.py:106
  211.2 6.0 %all_gather.26 = bf16[128,1024]{1,0:T(8,128)(2,1)S(1)} all-gather(bf16[128,256]{1,0:T(8,128)(2,1)} %reduce-scatter.4.cloned.1.call-done), channel_id=1, replica_groups=mesh['sp'=8,'tp'=4] {'tp'}, dimensions={1}, use_global_device_ids=true | all-gather | bytes 327680 | tf_op jit(solution)/shard_map/all_gather | solution.py:84
  217.4 1.3 fusion.15
  218.9 0.2 multiply_reduce_fusion.3
  219.3 1.3 convolution_convert_fusion.7
  220.9 3.4 %collective-permute-start.4 = (bf16[4,32,4,128]{3,1,2,0:T(8,128)(2,1)S(1)}, bf16[4,32,4,128]{3,1,2,0:T(8,128)(2,1)S(1)}, u32[]{:S(2)}, u32[]{:S(2)}) collective-permute-start(bf16[4,32,4,128]{3,1,2,0:T(8,128)(2,1)S(1)} %pad_maximum_fusion.4), channel_id=1, source_target_pairs={{0,4},{4,8},{8,12},{12,16},{16,20},{20,24},{24,28},{1,5},{5,9},{9,... | collective-permute-start | bytes 393224 | tf_op jit(solution)/shard_map/ppermute | solution.py:21
  224.3 1.5 collective-permute-start.5
  225.8 1.3 fusion.14
  227.2 0.2 multiply_reduce_fusion.2
  227.5 0.2 multiply_convert_fusion.1
  227.7 3.9 %collective-permute-done.5 = bf16[4,32,4,128]{3,1,2,0:T(8,128)(2,1)S(1)} collective-permute-done((bf16[4,32,4,128]{3,1,2,0:T(8,128)(2,1)S(1)}, bf16[4,32,4,128]{3,1,2,0:T(8,128)(2,1)S(1)}, u32[]{:S(2)}, u32[]{:S(2)}) %collective-permute-start.5) | collective-permute-done | bytes 131104 | tf_op jit(solution)/shard_map/ppermute | solution.py:22
  232.0 0.7 fusion.4
  232.7 0.6 fusion.1
  233.3 1.1 fusion.10
  234.6 2.0 convolution_convert_fusion.1
  236.7 3.5 %gather_fusion.2 = f32[1024,4,8]{2,1,0:T(4,128)S(1)} fusion(f32[4,8,16]{1,0,2:T(4,128)S(1)} %bitcast.250, s32[1024]{0:T(1024)S(1)} %broadcast_clamp_fusion), kind=kCustom, calls=%fused_computation.2 | custom fusion | bytes 266240 | tf_op jit(solution)/shard_map/gather | solution.py:55
  240.3 1.3 copy.184
  241.5 15.2 %reduce-scatter.6.cloned.1.call-done = bf16[128,256]{1,0:T(8,128)(2,1)} async-done(((bf16[128,1024]{1,0:T(8,128)(2,1)}), bf16[128,256]{1,0:T(8,128)(2,1)}) %reduce-scatter.6.cloned.1.call-update) | async-done | bytes 65552 | tf_op jit(solution)/shard_map/reduce_scatter | solution.py:106
  256.7 6.0 %all_gather.27 = bf16[128,1024]{1,0:T(8,128)(2,1)S(1)} all-gather(bf16[128,256]{1,0:T(8,128)(2,1)} %reduce-scatter.6.cloned.1.call-done), channel_id=1, replica_groups=mesh['sp'=8,'tp'=4] {'tp'}, dimensions={1}, use_global_device_ids=true | all-gather | bytes 327680 | tf_op jit(solution)/shard_map/all_gather | solution.py:84
  262.9 1.3 fusion.13
  264.3 0.2 multiply_reduce_fusion.1
  264.8 1.3 convolution_convert_fusion.4
  266.4 3.4 %collective-permute-start.6 = (bf16[4,32,4,128]{3,1,2,0:T(8,128)(2,1)S(1)}, bf16[4,32,4,128]{3,1,2,0:T(8,128)(2,1)S(1)}, u32[]{:S(2)}, u32[]{:S(2)}) collective-permute-start(bf16[4,32,4,128]{3,1,2,0:T(8,128)(2,1)S(1)} %pad_maximum_fusion.5), channel_id=1, source_target_pairs={{0,4},{4,8},{8,12},{12,16},{16,20},{20,24},{24,28},{1,5},{5,9},{9,... | collective-permute-start | bytes 393224 | tf_op jit(solution)/shard_map/ppermute | solution.py:21
  269.8 1.3 collective-permute-start.7
  271.1 1.3 fusion.12
  272.6 0.2 multiply_reduce_fusion
  272.8 0.2 multiply_convert_fusion
  273.1 4.1 %collective-permute-done.7 = bf16[4,32,4,128]{3,1,2,0:T(8,128)(2,1)S(1)} collective-permute-done((bf16[4,32,4,128]{3,1,2,0:T(8,128)(2,1)S(1)}, bf16[4,32,4,128]{3,1,2,0:T(8,128)(2,1)S(1)}, u32[]{:S(2)}, u32[]{:S(2)}) %collective-permute-start.7) | collective-permute-done | bytes 131104 | tf_op jit(solution)/shard_map/ppermute | solution.py:22
  277.5 0.7 fusion.5
  278.2 0.6 fusion.2
  278.8 1.1 fusion.9
  280.1 2.0 convolution_convert_fusion
  282.1 20.2 %reduce-scatter.8.cloned.1.call-done = bf16[128,256]{1,0:T(8,128)(2,1)} async-done(((bf16[128,1024]{1,0:T(8,128)(2,1)}), bf16[128,256]{1,0:T(8,128)(2,1)}) %reduce-scatter.8.cloned.1.call-update) | async-done | bytes 65552 | tf_op jit(solution)/shard_map/reduce_scatter | solution.py:106
  (101 shorter events, 5.2 us)
Async XLA Ops:
  6.5 49.9 %all-gather.5.cloned.1.call-start = ((), (), s32[]{:S(2)}) async-start(), calls=%async_computation.3 | async-start | bytes 1769472 | tf_op jit(solution)/shard_map/all_gather | solution.py:78
  7.3 93.9 %all-gather.7.cloned.1.call-start = ((), (), s32[]{:S(2)}) async-start(), calls=%async_computation.4 | async-start | bytes 1769472 | tf_op jit(solution)/shard_map/all_gather | solution.py:79
  8.0 137.9 %all-gather.9.cloned.1.call-start = ((), (), s32[]{:S(2)}) async-start(), calls=%async_computation.5 | async-start | bytes 1769472 | tf_op jit(solution)/shard_map/all_gather | solution.py:77
  8.7 181.9 %all-gather.11.cloned.1.call-start = ((), (), s32[]{:S(2)}) async-start(), calls=%async_computation.6 | async-start | bytes 1769472 | tf_op jit(solution)/shard_map/all_gather | solution.py:80
  9.5 19.1 %collective-permute-start.2 = (s32[4,32]{1,0:T(4,128)S(1)}, s32[4,32]{1,0:T(4,128)S(1)}, u32[]{:S(2)}, u32[]{:S(2)}) collective-permute-start(s32[4,32]{1,0:T(4,128)S(1)} %reshape.186), channel_id=1, source_target_pairs={{0,4},{4,8},{8,12},{12,16},{16,20},{20,24},{24,28},{1,5},{5,9},{9,... | collective-permute-start | bytes 1544 | tf_op jit(solution)/shard_map/ppermute | solution.py:21
  14.4 14.2 %collective-permute-start.3 = (s32[4,32]{1,0:T(4,128)S(1)}, s32[4,32]{1,0:T(4,128)S(1)}, u32[]{:S(2)}, u32[]{:S(2)}) collective-permute-start(s32[4,32]{1,0:T(4,128)S(1)} %reshape.186), channel_id=1, source_target_pairs={{4,0},{8,4},{12,8},{16,12},{20,16},{24,20},{28,24},{5,1},{9,5},{13... | collective-permute-start | bytes 1544 | tf_op jit(solution)/shard_map/ppermute | solution.py:22
  15.7 195.5 %reduce-scatter.4.cloned.1.call-start = ((), (), s32[]{:S(2)}) async-start(), calls=%async_computation.7 | async-start | bytes 327680 | tf_op jit(solution)/shard_map/reduce_scatter | solution.py:106
  102.8 45.1 %collective-permute-start = (bf16[4,32,4,128]{3,1,2,0:T(8,128)(2,1)S(1)}, bf16[4,32,4,128]{3,1,2,0:T(8,128)(2,1)S(1)}, u32[]{:S(2)}, u32[]{:S(2)}) collective-permute-start(bf16[4,32,4,128]{3,1,2,0:T(8,128)(2,1)S(1)} %pad_maximum_fusion.3), channel_id=1, source_target_pairs={{0,4},{4,8},{8,12},{12,16},{16,20},{20,24},{24,28},{1,5},{5,9},{9,... | collective-permute-start | bytes 393224 | tf_op jit(solution)/shard_map/ppermute | solution.py:21
  105.2 42.7 %collective-permute-start.1 = (bf16[4,32,4,128]{3,1,2,0:T(8,128)(2,1)S(1)}, bf16[4,32,4,128]{3,1,2,0:T(8,128)(2,1)S(1)}, u32[]{:S(2)}, u32[]{:S(2)}) collective-permute-start(bf16[4,32,4,128]{3,1,2,0:T(8,128)(2,1)S(1)} %pad_maximum_fusion.3), channel_id=1, source_target_pairs={{4,0},{8,4},{12,8},{16,12},{20,16},{24,20},{28,24},{5,1},{9,5},{13... | collective-permute-start | bytes 393224 | tf_op jit(solution)/shard_map/ppermute | solution.py:22
  192.7 64.1 %reduce-scatter.6.cloned.1.call-start = ((), (), s32[]{:S(2)}) async-start(), calls=%async_computation.8 | async-start | bytes 327680 | tf_op jit(solution)/shard_map/reduce_scatter | solution.py:106
  220.9 6.8 %collective-permute-start.4 = (bf16[4,32,4,128]{3,1,2,0:T(8,128)(2,1)S(1)}, bf16[4,32,4,128]{3,1,2,0:T(8,128)(2,1)S(1)}, u32[]{:S(2)}, u32[]{:S(2)}) collective-permute-start(bf16[4,32,4,128]{3,1,2,0:T(8,128)(2,1)S(1)} %pad_maximum_fusion.4), channel_id=1, source_target_pairs={{0,4},{4,8},{8,12},{12,16},{16,20},{20,24},{24,28},{1,5},{5,9},{9,... | collective-permute-start | bytes 393224 | tf_op jit(solution)/shard_map/ppermute | solution.py:21
  224.3 7.4 %collective-permute-start.5 = (bf16[4,32,4,128]{3,1,2,0:T(8,128)(2,1)S(1)}, bf16[4,32,4,128]{3,1,2,0:T(8,128)(2,1)S(1)}, u32[]{:S(2)}, u32[]{:S(2)}) collective-permute-start(bf16[4,32,4,128]{3,1,2,0:T(8,128)(2,1)S(1)} %pad_maximum_fusion.4), channel_id=1, source_target_pairs={{4,0},{8,4},{12,8},{16,12},{20,16},{24,20},{28,24},{5,1},{9,5},{13... | collective-permute-start | bytes 393224 | tf_op jit(solution)/shard_map/ppermute | solution.py:22
  236.6 65.7 %reduce-scatter.8.cloned.1.call-start = ((), (), s32[]{:S(2)}) async-start(), calls=%async_computation.9 | async-start | bytes 327680 | tf_op jit(solution)/shard_map/reduce_scatter | solution.py:106
  266.4 6.6 %collective-permute-start.6 = (bf16[4,32,4,128]{3,1,2,0:T(8,128)(2,1)S(1)}, bf16[4,32,4,128]{3,1,2,0:T(8,128)(2,1)S(1)}, u32[]{:S(2)}, u32[]{:S(2)}) collective-permute-start(bf16[4,32,4,128]{3,1,2,0:T(8,128)(2,1)S(1)} %pad_maximum_fusion.5), channel_id=1, source_target_pairs={{0,4},{4,8},{8,12},{12,16},{16,20},{20,24},{24,28},{1,5},{5,9},{9,... | collective-permute-start | bytes 393224 | tf_op jit(solution)/shard_map/ppermute | solution.py:21
  269.8 7.4 %collective-permute-start.7 = (bf16[4,32,4,128]{3,1,2,0:T(8,128)(2,1)S(1)}, bf16[4,32,4,128]{3,1,2,0:T(8,128)(2,1)S(1)}, u32[]{:S(2)}, u32[]{:S(2)}) collective-permute-start(bf16[4,32,4,128]{3,1,2,0:T(8,128)(2,1)S(1)} %pad_maximum_fusion.5), channel_id=1, source_target_pairs={{4,0},{8,4},{12,8},{16,12},{20,16},{24,20},{28,24},{5,1},{9,5},{13... | collective-permute-start | bytes 393224 | tf_op jit(solution)/shard_map/ppermute | solution.py:22
Sparse Core Ops, SparseCore 0:
  9.5 46.8 all-gather.4
  58.6 42.5 all-gather.6
  103.4 42.5 all-gather.8
  147.8 42.7 all-gather.10
  193.0 18.2 reduce-scatter.3
  236.7 19.9 reduce-scatter.5
  282.2 20.0 reduce-scatter.7
where the time goes:
time: 310 us; the launch traced here: 309 us
  waiting for transfers between devices  209 us (67%)
  matrix products  23 us (7%)
  starting transfers between devices  19.7 us (6%)
  local copies, waits for them, and re-layouts  19.3 us (6%)
  blocking collectives  17.9 us (6%)
  between operations  14.2 us (5%)
  other arithmetic  6.3 us (2%)
    reduce_scatter x3, waiting for transfers between devices, body(): lax.psum_scatter(partial_sums.astype(jnp.bfloat16), 'tp', scatter_dimensi...  49 us
    all_gather x1, waiting for transfers between devices, body(): lax.all_gather(w_value, 'sp', axis=1, tiled=True)  42.8 us
    all_gather x1, waiting for transfers between devices, body(): lax.all_gather(w_out, 'sp', axis=2, tiled=True)  39.8 us
    all_gather x1, waiting for transfers between devices, body(): lax.all_gather(w_query, 'sp', axis=1, tiled=True)  39.4 us
    all_gather x1, waiting for transfers between devices, body(): lax.all_gather(w_key, 'sp', axis=1, tiled=True)  27.4 us
    all_gather x3, blocking collectives, body(): gathered = lax.all_gather(stream, 'tp', axis=1, tiled=True)  17.9 us
    gather x6, local copies, waits for them, and re-layouts, attend(): bias_table = bias_layer[:, :, jnp.clip(col_offset, 0, WIN_COLS - 1)]  14.4 us
    ppermute x4, starting transfers between devices, with_halo(): before = lax.ppermute(last, axis, up)  14.1 us
  transfers between devices with their start and end apart: 15, of which 9 were waited for; matrix products, arithmetic and copies ran while one was open for 10% of the time, Pallas kernels for 0%

commit v1 on v0

--- a/solution.py
+++ b/solution.py
@@ -9,6 +9,18 @@
 LAYERS = 3
 GRID_W = 32
 EPS = 1e-06
+
+
+def ring_gather(shard, axis, dim):
+    ways, here, lap = (lax.axis_size(axis), lax.axis_index(axis), shard.shape[dim])
+    lengths = [n * ways if d == dim else n for d, n in enumerate(shard.shape)]
+    full = lax.dynamic_update_slice_in_dim(
+        jnp.zeros(lengths, shard.dtype), shard, here * lap, axis=dim
+    )
+    for far in range(1, ways):
+        shard = lax.ppermute(shard, axis, [(d, (d + 1) % ways) for d in range(ways)])
+        full = lax.dynamic_update_slice_in_dim(full, shard, (here - far) % ways * lap, axis=dim)
+    return full
 
 
 def with_halo(shard, sides, width, wrap):
@@ -77,7 +89,7 @@
         lax.all_gather(w_query, "sp", axis=1, tiled=True),
         lax.all_gather(w_key, "sp", axis=1, tiled=True),
         lax.all_gather(w_value, "sp", axis=1, tiled=True),
-        lax.all_gather(w_out, "sp", axis=2, tiled=True),
+        ring_gather(w_out, "sp", 2),
     )
     stream = tokens
     for layer_index in range(LAYERS):

time: 310 us -> 279 us (0.900)
  waiting for transfers between devices: 209 us -> 158 us
  local copies, waits for them, and re-layouts: 19.3 us -> 36.6 us
  starting transfers between devices: 19.7 us -> 25 us
  matrix products: 23 us -> 19.9 us
    ppermute x0 -> x7, waiting for transfers between devices: none -> 65.3 us  [ring_gather(): lax.ppermute(shard, axis, [(d, (d + 1) % ways) for d in range(ways)])]
    all_gather x1 -> x0, waiting for transfers between devices: 39.8 us -> none  [body(): lax.all_gather(w_out, 'sp', axis=2, tiled=True)]
    all_gather x1, waiting for transfers between devices: 42.8 us -> 4.04 us  [body(): lax.all_gather(w_value, 'sp', axis=1, tiled=True)]
    all_gather x1, waiting for transfers between devices: 27.4 us -> 0.02 us  [body(): lax.all_gather(w_key, 'sp', axis=1, tiled=True)]
    gather x6, local copies, waits for them, and re-layouts: 14.4 us -> 31 us  [attend(): bias_table = bias_layer[:, :, jnp.clip(col_offset, 0, WIN_COLS - 1)]]
    reduce_scatter x3, waiting for transfers between devices: 49 us -> 38 us  [body(): lax.psum_scatter(partial_sums.astype(jnp.bfloat16), 'tp', scatter_dimensi...]
    ppermute x0 -> x7, starting transfers between devices: none -> 5.88 us  [ring_gather(): lax.ppermute(shard, axis, [(d, (d + 1) % ways) for d in range(ways)])]
    dot_general x3, matrix products: 5.97 us -> 2.84 us  [body(): jnp.dot(attended, collected[3][layer_index], preferred_element_type=jnp.f...]
  transfers between devices with their start and end apart: 15 -> 21, of which waited for: 9 -> 13; matrix products, arithmetic and copies ran while one was open for 10% -> 16% of each run, Pallas kernels for 0% -> 0%
where the time goes in v1:
time: 279 us; the launch traced here: 278 us
  waiting for transfers between devices  158 us (57%)
  local copies, waits for them, and re-layouts  36.6 us (13%)
  starting transfers between devices  25 us (9%)
  matrix products  19.9 us (7%)
  blocking collectives  17.9 us (6%)
  between operations  14.4 us (5%)
  other arithmetic  6.29 us (2%)
    ppermute x7, waiting for transfers between devices, ring_gather(): lax.ppermute(shard, axis, [(d, (d + 1) % ways) for d in range(ways)])  65.3 us
    all_gather x1, waiting for transfers between devices, body(): lax.all_gather(w_query, 'sp', axis=1, tiled=True)  40.8 us
    reduce_scatter x3, waiting for transfers between devices, body(): lax.psum_scatter(partial_sums.astype(jnp.bfloat16), 'tp', scatter_dimensi...  38 us
    gather x6, local copies, waits for them, and re-layouts, attend(): bias_table = bias_layer[:, :, jnp.clip(col_offset, 0, WIN_COLS - 1)]  31 us
    all_gather x3, blocking collectives, body(): gathered = lax.all_gather(stream, 'tp', axis=1, tiled=True)  17.9 us
    ppermute x4, starting transfers between devices, with_halo(): before = lax.ppermute(last, axis, up)  13.6 us
    ppermute x4, waiting for transfers between devices, with_halo(): after = lax.ppermute(leading, axis, down)  8.01 us
    ppermute x7, starting transfers between devices, ring_gather(): lax.ppermute(shard, axis, [(d, (d + 1) % ways) for d in range(ways)])  5.88 us
  transfers between devices with their start and end apart: 21, of which 13 were waited for; matrix products, arithmetic and copies ran while one was open for 16% of the time, Pallas kernels for 0%

profile of v1, /device:TPU:0, one launch (start us, length us, event | category | flops | bytes accessed | tf_op | source)
XLA Modules:
  0.0 277.8 jit_solution(13242562288782460515)
XLA Ops:
  6.5 0.7 all-gather.4.cloned.1.call-update
  7.3 0.7 all-gather.6.cloned.1.call-update
  8.1 0.7 broadcast_add_fusion
  8.8 4.9 %collective-permute-start.2 = (s32[4,32]{1,0:T(4,128)S(1)}, s32[4,32]{1,0:T(4,128)S(1)}, u32[]{:S(2)}, u32[]{:S(2)}) collective-permute-start(s32[4,32]{1,0:T(4,128)S(1)} %reshape.186), channel_id=1, source_target_pairs={{0,4},{4,8},{8,12},{12,16},{16,20},{20,24},{24,28},{1,5},{5,9},{9,... | collective-permute-start | bytes 1544 | tf_op jit(solution)/shard_map/ppermute | solution.py:33
  13.7 1.3 collective-permute-start.3
  15.0 2.7 collective-permute-start.4
  18.0 6.0 %all_gather.18 = bf16[128,1024]{1,0:T(8,128)(2,1)S(1)} all-gather(bf16[128,256]{1,0:T(8,128)(2,1)} %param.8), channel_id=1, replica_groups=mesh['sp'=8,'tp'=4] {'tp'}, dimensions={1}, use_global_device_ids=true | all-gather | bytes 327680 | tf_op jit(solution)/shard_map/all_gather | solution.py:96
  24.1 0.8 fusion.79
  25.0 0.8 fusion.78
  26.2 7.9 %gather_fusion = f32[1024,4,8]{2,1,0:T(4,128)} fusion(f32[4,8,16]{1,0,2:T(4,128)S(1)} %bitcast.250, s32[1024]{0:T(1024)S(1)} %broadcast_clamp_fusion), kind=kCustom, calls=%fused_computation | custom fusion | bytes 266240 | tf_op jit(solution)/shard_map/gather | solution.py:67
  34.1 2.4 copy.150
  36.7 2.5 collective-permute-start.5
  39.2 11.1 %collective-permute-done.5 = bf16[3,256,128]{2,1,0:T(8,128)(2,1)S(1)} collective-permute-done((bf16[3,256,128]{2,1,0:T(8,128)(2,1)S(1)}, bf16[3,256,128]{2,1,0:T(8,128)(2,1)S(1)}, u32[]{:S(2)}, u32[]{:S(2)}) %collective-permute-start.5) | collective-permute-done | bytes 196640 | tf_op jit(solution)/shard_map/ppermute | solution.py:21
  50.2 0.7 collective-permute-start.6
  50.9 12.1 %collective-permute-done.6 = bf16[3,256,128]{2,1,0:T(8,128)(2,1)S(1)} collective-permute-done((bf16[3,256,128]{2,1,0:T(8,128)(2,1)S(1)}, bf16[3,256,128]{2,1,0:T(8,128)(2,1)S(1)}, u32[]{:S(2)}, u32[]{:S(2)}) %collective-permute-start.6) | collective-permute-done | bytes 196640 | tf_op jit(solution)/shard_map/ppermute | solution.py:21
  63.3 8.2 %collective-permute-done.7 = bf16[3,256,128]{2,1,0:T(8,128)(2,1)S(1)} collective-permute-done((bf16[3,256,128]{2,1,0:T(8,128)(2,1)S(1)}, bf16[3,256,128]{2,1,0:T(8,128)(2,1)S(1)}, u32[]{:S(2)}, u32[]{:S(2)}) %collective-permute-start.7) | collective-permute-done | bytes 196640 | tf_op jit(solution)/shard_map/ppermute | solution.py:21
  71.6 13.2 %collective-permute-done.8 = bf16[3,256,128]{2,1,0:T(8,128)(2,1)S(1)} collective-permute-done((bf16[3,256,128]{2,1,0:T(8,128)(2,1)S(1)}, bf16[3,256,128]{2,1,0:T(8,128)(2,1)S(1)}, u32[]{:S(2)}, u32[]{:S(2)}) %collective-permute-start.8) | collective-permute-done | bytes 196640 | tf_op jit(solution)/shard_map/ppermute | solution.py:21
  85.0 8.6 %collective-permute-done.9 = bf16[3,256,128]{2,1,0:T(8,128)(2,1)S(1)} collective-permute-done((bf16[3,256,128]{2,1,0:T(8,128)(2,1)S(1)}, bf16[3,256,128]{2,1,0:T(8,128)(2,1)S(1)}, u32[]{:S(2)}, u32[]{:S(2)}) %collective-permute-start.9) | collective-permute-done | bytes 196640 | tf_op jit(solution)/shard_map/ppermute | solution.py:21
  93.7 12.1 %collective-permute-done.10 = bf16[3,256,128]{2,1,0:T(8,128)(2,1)S(1)} collective-permute-done((bf16[3,256,128]{2,1,0:T(8,128)(2,1)S(1)}, bf16[3,256,128]{2,1,0:T(8,128)(2,1)S(1)}, u32[]{:S(2)}, u32[]{:S(2)}) %collective-permute-start.10) | collective-permute-done | bytes 196640 | tf_op jit(solution)/shard_map/ppermute | solution.py:21
  105.9 1.3 fusion.17
  107.4 0.2 multiply_reduce_fusion.5
  107.7 4.0 %all-gather.6.cloned.1.call-done = bf16[3,1024,256]{2,1,0:T(8,128)(2,1)} async-done(((bf16[3,128,256]{2,1,0:T(8,128)(2,1)}), bf16[3,1024,256]{2,1,0:T(8,128)(2,1)}) %all-gather.6.cloned.1.call-update) | async-done | bytes 1572880 | tf_op jit(solution)/shard_map/all_gather | solution.py:91
  111.7 1.3 convolution_convert_fusion.10
  113.5 1.9 collective-permute-start
  115.4 1.3 collective-permute-start.1
  116.7 40.8 %all-gather.8.cloned.1.call-done = bf16[3,1024,256]{2,1,0:T(8,128)(2,1)} async-done(((bf16[3,128,256]{2,1,0:T(8,128)(2,1)}), bf16[3,1024,256]{2,1,0:T(8,128)(2,1)}) %all-gather.8.cloned.1.call-update) | async-done | bytes 1572880 | tf_op jit(solution)/shard_map/all_gather | solution.py:89
  157.5 1.3 fusion.16
  159.0 0.2 multiply_reduce_fusion.4
  159.9 0.7 fusion.3
  160.5 0.6 fusion
  161.1 1.1 fusion.11
  162.4 1.0 convolution_convert_fusion.2
  163.5 8.0 %gather_fusion.1 = f32[1024,4,8]{2,1,0:T(4,128)} fusion(f32[4,8,16]{1,0,2:T(4,128)S(1)} %bitcast.252, s32[1024]{0:T(1024)S(1)} %broadcast_clamp_fusion), kind=kCustom, calls=%fused_computation.1 | custom fusion | bytes 266240 | tf_op jit(solution)/shard_map/gather | solution.py:67
  171.5 2.4 copy.167
  173.9 8.1 %reduce-scatter.4.cloned.1.call-done = bf16[128,256]{1,0:T(8,128)(2,1)} async-done(((bf16[128,1024]{1,0:T(8,128)(2,1)}), bf16[128,256]{1,0:T(8,128)(2,1)}) %reduce-scatter.4.cloned.1.call-update) | async-done | bytes 65552 | tf_op jit(solution)/shard_map/reduce_scatter | solution.py:118
  182.0 6.0 %all_gather.22 = bf16[128,1024]{1,0:T(8,128)(2,1)S(1)} all-gather(bf16[128,256]{1,0:T(8,128)(2,1)} %reduce-scatter.4.cloned.1.call-done), channel_id=1, replica_groups=mesh['sp'=8,'tp'=4] {'tp'}, dimensions={1}, use_global_device_ids=true | all-gather | bytes 327680 | tf_op jit(solution)/shard_map/all_gather | solution.py:96
  188.1 1.3 fusion.15
  189.6 0.2 multiply_reduce_fusion.3
  190.1 1.3 convolution_convert_fusion.7
  191.7 3.4 %collective-permute-start.11 = (bf16[4,32,4,128]{3,1,2,0:T(8,128)(2,1)S(1)}, bf16[4,32,4,128]{3,1,2,0:T(8,128)(2,1)S(1)}, u32[]{:S(2)}, u32[]{:S(2)}) collective-permute-start(bf16[4,32,4,128]{3,1,2,0:T(8,128)(2,1)S(1)} %pad_maximum_fusion.4), channel_id=1, source_target_pairs={{0,4},{4,8},{8,12},{12,16},{16,20},{20,24},{24,28},{1,5},{5,9},{9,... | collective-permute-start | bytes 393224 | tf_op jit(solution)/shard_map/ppermute | solution.py:33
  195.1 1.5 collective-permute-start.12
  196.5 1.3 fusion.14
  198.0 0.2 multiply_reduce_fusion.2
  198.5 3.9 %collective-permute-done.12 = bf16[4,32,4,128]{3,1,2,0:T(8,128)(2,1)S(1)} collective-permute-done((bf16[4,32,4,128]{3,1,2,0:T(8,128)(2,1)S(1)}, bf16[4,32,4,128]{3,1,2,0:T(8,128)(2,1)S(1)}, u32[]{:S(2)}, u32[]{:S(2)}) %collective-permute-start.12) | collective-permute-done | bytes 131104 | tf_op jit(solution)/shard_map/ppermute | solution.py:34
  202.8 0.7 fusion.4
  203.4 0.6 fusion.1
  204.0 1.1 fusion.10
  205.3 1.0 convolution_convert_fusion.1
  206.4 8.0 %gather_fusion.2 = f32[1024,4,8]{2,1,0:T(4,128)} fusion(f32[4,8,16]{1,0,2:T(4,128)S(1)} %bitcast.251, s32[1024]{0:T(1024)S(1)} %broadcast_clamp_fusion), kind=kCustom, calls=%fused_computation.2 | custom fusion | bytes 266240 | tf_op jit(solution)/shard_map/gather | solution.py:67
  214.4 2.4 copy.184
  216.8 9.7 %reduce-scatter.6.cloned.1.call-done = bf16[128,256]{1,0:T(8,128)(2,1)} async-done(((bf16[128,1024]{1,0:T(8,128)(2,1)}), bf16[128,256]{1,0:T(8,128)(2,1)}) %reduce-scatter.6.cloned.1.call-update) | async-done | bytes 65552 | tf_op jit(solution)/shard_map/reduce_scatter | solution.py:118
  226.5 6.0 %all_gather.23 = bf16[128,1024]{1,0:T(8,128)(2,1)S(1)} all-gather(bf16[128,256]{1,0:T(8,128)(2,1)} %reduce-scatter.6.cloned.1.call-done), channel_id=1, replica_groups=mesh['sp'=8,'tp'=4] {'tp'}, dimensions={1}, use_global_device_ids=true | all-gather | bytes 327680 | tf_op jit(solution)/shard_map/all_gather | solution.py:96
  232.6 1.3 fusion.13
  234.6 1.3 convolution_convert_fusion.4
  236.2 3.4 %collective-permute-start.13 = (bf16[4,32,4,128]{3,1,2,0:T(8,128)(2,1)S(1)}, bf16[4,32,4,128]{3,1,2,0:T(8,128)(2,1)S(1)}, u32[]{:S(2)}, u32[]{:S(2)}) collective-permute-start(bf16[4,32,4,128]{3,1,2,0:T(8,128)(2,1)S(1)} %pad_maximum_fusion.5), channel_id=1, source_target_pairs={{0,4},{4,8},{8,12},{12,16},{16,20},{20,24},{24,28},{1,5},{5,9},{9,... | collective-permute-start | bytes 393224 | tf_op jit(solution)/shard_map/ppermute | solution.py:33
  239.6 1.3 collective-permute-start.14
  240.9 1.3 fusion.12
  242.3 0.2 multiply_reduce_fusion
  242.8 4.1 %collective-permute-done.14 = bf16[4,32,4,128]{3,1,2,0:T(8,128)(2,1)S(1)} collective-permute-done((bf16[4,32,4,128]{3,1,2,0:T(8,128)(2,1)S(1)}, bf16[4,32,4,128]{3,1,2,0:T(8,128)(2,1)S(1)}, u32[]{:S(2)}, u32[]{:S(2)}) %collective-permute-start.14) | collective-permute-done | bytes 131104 | tf_op jit(solution)/shard_map/ppermute | solution.py:34
  247.3 0.7 fusion.5
  247.9 0.6 fusion.2
  248.5 1.1 fusion.9
  249.8 0.9 convolution_convert_fusion
  250.8 20.2 %reduce-scatter.8.cloned.1.call-done = bf16[128,256]{1,0:T(8,128)(2,1)} async-done(((bf16[128,1024]{1,0:T(8,128)(2,1)}), bf16[128,256]{1,0:T(8,128)(2,1)}) %reduce-scatter.8.cloned.1.call-update) | async-done | bytes 65552 | tf_op jit(solution)/shard_map/reduce_scatter | solution.py:118
  (123 shorter events, 7.1 us)
Async XLA Ops:
  6.5 19.6 %copy-start = (bf16[3,256,128]{2,1,0:T(8,128)(2,1)S(1)}, bf16[3,256,128]{2,1,0:T(8,128)(2,1)}, u32[]{:S(2)}) copy-start(bf16[3,256,128]{2,1,0:T(8,128)(2,1)} %param.13) | copy-start | bytes 589828
  6.5 99.3 %all-gather.4.cloned.1.call-start = ((), (), s32[]{:S(2)}) async-start(), calls=%async_computation.3 | async-start | bytes 1769472 | tf_op jit(solution)/shard_map/all_gather | solution.py:90
  7.3 104.5 %all-gather.6.cloned.1.call-start = ((), (), s32[]{:S(2)}) async-start(), calls=%async_computation.4 | async-start | bytes 1769472 | tf_op jit(solution)/shard_map/all_gather | solution.py:91
  8.0 149.5 %all-gather.8.cloned.1.call-start = ((), (), s32[]{:S(2)}) async-start(), calls=%async_computation.5 | async-start | bytes 1769472 | tf_op jit(solution)/shard_map/all_gather | solution.py:89
  8.8 27.7 %collective-permute-start.2 = (s32[4,32]{1,0:T(4,128)S(1)}, s32[4,32]{1,0:T(4,128)S(1)}, u32[]{:S(2)}, u32[]{:S(2)}) collective-permute-start(s32[4,32]{1,0:T(4,128)S(1)} %reshape.186), channel_id=1, source_target_pairs={{0,4},{4,8},{8,12},{12,16},{16,20},{20,24},{24,28},{1,5},{5,9},{9,... | collective-permute-start | bytes 1544 | tf_op jit(solution)/shard_map/ppermute | solution.py:33
  13.7 22.9 %collective-permute-start.3 = (s32[4,32]{1,0:T(4,128)S(1)}, s32[4,32]{1,0:T(4,128)S(1)}, u32[]{:S(2)}, u32[]{:S(2)}) collective-permute-start(s32[4,32]{1,0:T(4,128)S(1)} %reshape.186), channel_id=1, source_target_pairs={{4,0},{8,4},{12,8},{16,12},{20,16},{24,20},{28,24},{5,1},{9,5},{13... | collective-permute-start | bytes 1544 | tf_op jit(solution)/shard_map/ppermute | solution.py:34
  15.0 21.7 %collective-permute-start.4 = (bf16[3,256,128]{2,1,0:T(8,128)(2,1)}, bf16[3,256,128]{2,1,0:T(8,128)(2,1)S(1)}, u32[]{:S(2)}, u32[]{:S(2)}) collective-permute-start(bf16[3,256,128]{2,1,0:T(8,128)(2,1)} %param.13), channel_id=1, source_target_pairs={{0,4},{4,8},{8,12},{12,16},{16,20},{20,24},{24,28},{28,0},{1,5},{5... | collective-permute-start | bytes 589832 | tf_op jit(solution)/shard_map/ppermute | solution.py:21
  17.7 164.3 %reduce-scatter.4.cloned.1.call-start = ((), (), s32[]{:S(2)}) async-start(), calls=%async_computation.6 | async-start | bytes 327680 | tf_op jit(solution)/shard_map/reduce_scatter | solution.py:118
  36.7 13.6 %collective-permute-start.5 = (bf16[3,256,128]{2,1,0:T(8,128)(2,1)S(1)}, bf16[3,256,128]{2,1,0:T(8,128)(2,1)S(1)}, u32[]{:S(2)}, u32[]{:S(2)}) collective-permute-start(bf16[3,256,128]{2,1,0:T(8,128)(2,1)S(1)} %collective-permute-done.4), channel_id=1, source_target_pairs={{0,4},{4,8},{8,12},{12,16},{16,20},{20,24},{24,28},{28,0},{1,5},{5... | collective-permute-start | bytes 589832 | tf_op jit(solution)/shard_map/ppermute | solution.py:21
  50.2 12.8 %collective-permute-start.6 = (bf16[3,256,128]{2,1,0:T(8,128)(2,1)S(1)}, bf16[3,256,128]{2,1,0:T(8,128)(2,1)S(1)}, u32[]{:S(2)}, u32[]{:S(2)}) collective-permute-start(bf16[3,256,128]{2,1,0:T(8,128)(2,1)S(1)} %collective-permute-done.5), channel_id=1, source_target_pairs={{0,4},{4,8},{8,12},{12,16},{16,20},{20,24},{24,28},{28,0},{1,5},{5... | collective-permute-start | bytes 589832 | tf_op jit(solution)/shard_map/ppermute | solution.py:21
  63.1 8.4 %collective-permute-start.7 = (bf16[3,256,128]{2,1,0:T(8,128)(2,1)S(1)}, bf16[3,256,128]{2,1,0:T(8,128)(2,1)S(1)}, u32[]{:S(2)}, u32[]{:S(2)}) collective-permute-start(bf16[3,256,128]{2,1,0:T(8,128)(2,1)S(1)} %collective-permute-done.6), channel_id=1, source_target_pairs={{0,4},{4,8},{8,12},{12,16},{16,20},{20,24},{24,28},{28,0},{1,5},{5... | collective-permute-start | bytes 589832 | tf_op jit(solution)/shard_map/ppermute | solution.py:21
  71.4 13.4 %collective-permute-start.8 = (bf16[3,256,128]{2,1,0:T(8,128)(2,1)S(1)}, bf16[3,256,128]{2,1,0:T(8,128)(2,1)S(1)}, u32[]{:S(2)}, u32[]{:S(2)}) collective-permute-start(bf16[3,256,128]{2,1,0:T(8,128)(2,1)S(1)} %collective-permute-done.7), channel_id=1, source_target_pairs={{0,4},{4,8},{8,12},{12,16},{16,20},{20,24},{24,28},{28,0},{1,5},{5... | collective-permute-start | bytes 589832 | tf_op jit(solution)/shard_map/ppermute | solution.py:21
  84.8 8.8 %collective-permute-start.9 = (bf16[3,256,128]{2,1,0:T(8,128)(2,1)S(1)}, bf16[3,256,128]{2,1,0:T(8,128)(2,1)S(1)}, u32[]{:S(2)}, u32[]{:S(2)}) collective-permute-start(bf16[3,256,128]{2,1,0:T(8,128)(2,1)S(1)} %collective-permute-done.8), channel_id=1, source_target_pairs={{0,4},{4,8},{8,12},{12,16},{16,20},{20,24},{24,28},{28,0},{1,5},{5... | collective-permute-start | bytes 589832 | tf_op jit(solution)/shard_map/ppermute | solution.py:21
  93.6 12.2 %collective-permute-start.10 = (bf16[3,256,128]{2,1,0:T(8,128)(2,1)S(1)}, bf16[3,256,128]{2,1,0:T(8,128)(2,1)S(1)}, u32[]{:S(2)}, u32[]{:S(2)}) collective-permute-start(bf16[3,256,128]{2,1,0:T(8,128)(2,1)S(1)} %collective-permute-done.9), channel_id=1, source_target_pairs={{0,4},{4,8},{8,12},{12,16},{16,20},{20,24},{24,28},{28,0},{1,5},{5... | collective-permute-start | bytes 589832 | tf_op jit(solution)/shard_map/ppermute | solution.py:21
  113.5 46.0 %collective-permute-start = (bf16[4,32,4,128]{3,1,2,0:T(8,128)(2,1)S(1)}, bf16[4,32,4,128]{3,1,2,0:T(8,128)(2,1)S(1)}, u32[]{:S(2)}, u32[]{:S(2)}) collective-permute-start(bf16[4,32,4,128]{3,1,2,0:T(8,128)(2,1)S(1)} %pad_maximum_fusion.3), channel_id=1, source_target_pairs={{0,4},{4,8},{8,12},{12,16},{16,20},{20,24},{24,28},{1,5},{5,9},{9,... | collective-permute-start | bytes 393224 | tf_op jit(solution)/shard_map/ppermute | solution.py:33
  115.4 44.1 %collective-permute-start.1 = (bf16[4,32,4,128]{3,1,2,0:T(8,128)(2,1)S(1)}, bf16[4,32,4,128]{3,1,2,0:T(8,128)(2,1)S(1)}, u32[]{:S(2)}, u32[]{:S(2)}) collective-permute-start(bf16[4,32,4,128]{3,1,2,0:T(8,128)(2,1)S(1)} %pad_maximum_fusion.3), channel_id=1, source_target_pairs={{4,0},{8,4},{12,8},{16,12},{20,16},{24,20},{28,24},{5,1},{9,5},{13... | collective-permute-start | bytes 393224 | tf_op jit(solution)/shard_map/ppermute | solution.py:34
  163.4 63.1 %reduce-scatter.6.cloned.1.call-start = ((), (), s32[]{:S(2)}) async-start(), calls=%async_computation.7 | async-start | bytes 327680 | tf_op jit(solution)/shard_map/reduce_scatter | solution.py:118
  191.7 6.8 %collective-permute-start.11 = (bf16[4,32,4,128]{3,1,2,0:T(8,128)(2,1)S(1)}, bf16[4,32,4,128]{3,1,2,0:T(8,128)(2,1)S(1)}, u32[]{:S(2)}, u32[]{:S(2)}) collective-permute-start(bf16[4,32,4,128]{3,1,2,0:T(8,128)(2,1)S(1)} %pad_maximum_fusion.4), channel_id=1, source_target_pairs={{0,4},{4,8},{8,12},{12,16},{16,20},{20,24},{24,28},{1,5},{5,9},{9,... | collective-permute-start | bytes 393224 | tf_op jit(solution)/shard_map/ppermute | solution.py:33
  195.1 7.4 %collective-permute-start.12 = (bf16[4,32,4,128]{3,1,2,0:T(8,128)(2,1)S(1)}, bf16[4,32,4,128]{3,1,2,0:T(8,128)(2,1)S(1)}, u32[]{:S(2)}, u32[]{:S(2)}) collective-permute-start(bf16[4,32,4,128]{3,1,2,0:T(8,128)(2,1)S(1)} %pad_maximum_fusion.4), channel_id=1, source_target_pairs={{4,0},{8,4},{12,8},{16,12},{20,16},{24,20},{28,24},{5,1},{9,5},{13... | collective-permute-start | bytes 393224 | tf_op jit(solution)/shard_map/ppermute | solution.py:34
  206.3 64.7 %reduce-scatter.8.cloned.1.call-start = ((), (), s32[]{:S(2)}) async-start(), calls=%async_computation.8 | async-start | bytes 327680 | tf_op jit(solution)/shard_map/reduce_scatter | solution.py:118
  236.2 6.6 %collective-permute-start.13 = (bf16[4,32,4,128]{3,1,2,0:T(8,128)(2,1)S(1)}, bf16[4,32,4,128]{3,1,2,0:T(8,128)(2,1)S(1)}, u32[]{:S(2)}, u32[]{:S(2)}) collective-permute-start(bf16[4,32,4,128]{3,1,2,0:T(8,128)(2,1)S(1)} %pad_maximum_fusion.5), channel_id=1, source_target_pairs={{0,4},{4,8},{8,12},{12,16},{16,20},{20,24},{24,28},{1,5},{5,9},{9,... | collective-permute-start | bytes 393224 | tf_op jit(solution)/shard_map/ppermute | solution.py:33
  239.6 7.4 %collective-permute-start.14 = (bf16[4,32,4,128]{3,1,2,0:T(8,128)(2,1)S(1)}, bf16[4,32,4,128]{3,1,2,0:T(8,128)(2,1)S(1)}, u32[]{:S(2)}, u32[]{:S(2)}) collective-permute-start(bf16[4,32,4,128]{3,1,2,0:T(8,128)(2,1)S(1)} %pad_maximum_fusion.5), channel_id=1, source_target_pairs={{4,0},{8,4},{12,8},{16,12},{20,16},{24,20},{28,24},{5,1},{9,5},{13... | collective-permute-start | bytes 393224 | tf_op jit(solution)/shard_map/ppermute | solution.py:34
Sparse Core Ops, SparseCore 0:
  9.5 52.0 all-gather.3
  63.8 47.9 all-gather.5
  113.9 43.5 all-gather.7
  163.5 18.4 reduce-scatter.3
  206.4 20.0 reduce-scatter.5
  250.9 20.0 reduce-scatter.7
